TPU v7x, 32 devices: a whole 2x2x4 slice. The times are simulated.
32 devices in a mesh: tp: 8 (over z, y), dp: 4 (over x, core).
Axes of the slice: x: 2, y: 2, z: 4, core: 2. Of those that a mesh axis runs over, the one named last changes fastest.
Arguments:
- residual: bfloat16 [128, 4096], P(None, ('dp', 'tp')), may hold values from -50 to 50, as said below
- norm_gain: bfloat16 [2, 4096], P(None, ('dp', 'tp')), may hold values from 0.099609375 to 1.8984375
- w_query: bfloat16 [2, 4096, 4096], P(None, 'dp', 'tp'), may hold values from -0.09375 to 0.09375
- w_forget: bfloat16 [2, 4096, 4096], P(None, 'dp', 'tp'), may hold values from -0.09375 to 0.09375
- w_value: bfloat16 [2, 4096, 4096], P(None, 'dp', 'tp'), may hold values from -0.09375 to 0.09375
- w_output_gate: bfloat16 [2, 4096, 4096], P(None, 'dp', 'tp'), may hold values from -0.09375 to 0.09375
- lower_bound: float32 [2, 4096], P(None, 'tp'), may hold values from 0 to 0.9
- head_gain: bfloat16 [2, 4096], P(None, 'tp'), may hold values from 0.099609375 to 1.8984375
- w_out: bfloat16 [2, 4096, 4096], P(None, 'tp', 'dp'), may hold values from -0.125 to 0.125
- state: float32 [2, 128, 32, 128, 128], P(None, 'dp', 'tp'), may hold values from -2.4 to 2.4
Outputs:
- new_residual: bfloat16 [128, 4096], P(None, ('dp', 'tp'))
- new_state: float32 [2, 128, 32, 128, 128], P(None, 'dp', 'tp')
Inputs may be any that keep to these rules, and one draw needn't show every extreme that they name: residual rows of normal entries, each group of 16 consecutive features with its own scale.
All inputs are finite; a program needn't handle non-finite values.
Results may differ from a plain program's by a relative error of at most 0.02.
Values may be sent and summed in bfloat16 or wider, within the bound.
A program may use at most 128 MiB of HBM per device.

v0:
```python
import functools

import jax
import jax.numpy as jnp
from jax import lax
from jax.experimental import pallas as pl
from jax.experimental.pallas import tpu as pltpu
from jax.sharding import PartitionSpec as P

D = 4096
HEAD_DIM = 128
BLOCKS = 2


norm_eps = 1e-06


def one_block(x, gain, w_q, w_f, w_v, w_g, bound, h_gain, w_o, old_state):
    xf = x.astype(jnp.float32)
    x_whole, g_whole = (
        lax.all_gather(x, "tp", axis=1, tiled=True),
        lax.all_gather(gain, "tp", axis=1, tiled=True),
    )
    x_wide = x_whole.astype(jnp.float32)
    scaled = (x_wide * g_whole.astype(jnp.float32)).astype(jnp.bfloat16)
    part_q = jnp.dot(scaled, w_q, preferred_element_type=jnp.float32)
    part_f = jnp.dot(scaled, w_f, preferred_element_type=jnp.float32)
    part_v = jnp.dot(scaled, w_v, preferred_element_type=jnp.float32)
    part_g = jnp.dot(scaled, w_g, preferred_element_type=jnp.float32)
    total_sq = lax.psum(jnp.sum(x_wide * x_wide, axis=1), "dp")
    pq, pf, pv, pg = (
        lax.psum_scatter(part_q.astype(jnp.bfloat16), "dp", scatter_dimension=0, tiled=True).astype(
            jnp.float32
        ),
        lax.psum_scatter(part_f.astype(jnp.bfloat16), "dp", scatter_dimension=0, tiled=True).astype(
            jnp.float32
        ),
        lax.psum_scatter(part_v.astype(jnp.bfloat16), "dp", scatter_dimension=0, tiled=True).astype(
            jnp.float32
        ),
        lax.psum_scatter(part_g.astype(jnp.bfloat16), "dp", scatter_dimension=0, tiled=True).astype(
            jnp.float32
        ),
    )
    own = pq.shape[0]
    own_sq = lax.dynamic_slice_in_dim(total_sq, lax.axis_index("dp") * own, own, 0)
    scale = lax.rsqrt(own_sq / D + norm_eps)[:, None]

    def finish(total):
        return lax.optimization_barrier((total * scale).astype(jnp.bfloat16)).astype(jnp.float32)

    pq, pf, pv, pg = (finish(pq), finish(pf), finish(pv), finish(pg))
    heads_here = old_state.shape[1]
    query = jax.nn.silu(pq).reshape(own, heads_here, HEAD_DIM)
    forget = (bound + (1.0 - bound) * jax.nn.sigmoid(pf)).reshape(own, heads_here, HEAD_DIM)
    key = ((1.0 - bound) * jax.nn.sigmoid(-pf)).reshape(own, heads_here, HEAD_DIM)
    value = pv.reshape(own, heads_here, HEAD_DIM)
    fresh = forget[..., None] * old_state + key[..., None] * value[:, :, None, :]
    read = jnp.einsum("bhk,bhkv->bhv", query, fresh)
    normed = read * lax.rsqrt(jnp.mean(read * read, axis=2, keepdims=True) + norm_eps)
    normed = normed.reshape(own, heads_here * HEAD_DIM) * h_gain.astype(jnp.float32)
    hidden = (normed * jax.nn.silu(pg)).astype(jnp.bfloat16)
    terms = jnp.dot(
        lax.all_gather(hidden, "dp", axis=0, tiled=True), w_o, preferred_element_type=jnp.float32
    )
    mixed = lax.psum_scatter(
        terms.astype(jnp.bfloat16), "tp", scatter_dimension=1, tiled=True
    ).astype(jnp.float32)
    return ((xf + mixed).astype(jnp.bfloat16), fresh)


def body(
    residual,
    norm_gain,
    w_query,
    w_forget,
    w_value,
    w_output_gate,
    lower_bound,
    head_gain,
    w_out,
    state,
):
    current = residual
    states = []
    for layer in range(BLOCKS):
        current, fresh = one_block(
            current,
            norm_gain[layer : layer + 1],
            w_query[layer],
            w_forget[layer],
            w_value[layer],
            w_output_gate[layer],
            lower_bound[layer],
            head_gain[layer],
            w_out[layer],
            state[layer],
        )
        states.append(fresh)
    return (current, jnp.stack(states))


LANES = 128
ROLES = 4
F32 = jnp.float32
BF16 = jnp.bfloat16


def silu(v):
    return v / (1.0 + jnp.exp(-v))


def sigmoid(v):
    return 1.0 / (1.0 + jnp.exp(-v))


def step_kernel(
    n_tp, n_dp,
    x_ref, gain_ref, bound_ref, h_gain_ref, wq_hbm, wf_hbm, wv_hbm, wg_hbm, wo_hbm, state_hbm,
    out_ref, forget_ref, value_ref,
    w_buf, wo_buf, s_buf, xg, gg, scaled, ss_buf, ss_recv, part, pair_recv, mid, part_recv, coef, read, hg,
    terms, pair_terms, mid_terms, terms_recv,
    load_sem, x_send, x_recv, g_send, g_recv, ss_send, ss_recv_sem, q_send, q_recv, p_send, p_recv,
    h_send, h_recv, y_send, y_recv, t_send, t_recv,
):
    me_t, me_d = lax.axis_index("tp"), lax.axis_index("dp")
    batch, feats = x_ref.shape
    own = batch // n_dp
    heads = s_buf.shape[2]

    n_z, n_x = n_tp // 2, n_dp // 2
    pair_t = me_t + 1 - 2 * lax.rem(me_t, 2)
    pair_d = me_d + 1 - 2 * lax.rem(me_d, 2)

    def along_z(t, k):
        return lax.rem(t + 2 * k + n_tp, n_tp)

    def along_x(d, k):
        return lax.rem(d + 2 * k + n_dp, n_dp)

    def dp_peer(k):
        return lax.rem(me_d + k, n_dp)

    loads = []
    for b in range(BLOCKS):
        group = [
            pltpu.make_async_copy(w.at[b], w_buf.at[b, r], load_sem.at[b, r])
            for r, w in enumerate((wq_hbm, wf_hbm, wv_hbm, wg_hbm))
        ]
        group.append(pltpu.make_async_copy(state_hbm.at[b], s_buf.at[b], load_sem.at[b, 4]))
        group.append(pltpu.make_async_copy(wo_hbm.at[b], wo_buf.at[b], load_sem.at[b, 5]))
        for c in group:
            c.start()
        loads.append(group)

    barrier = pltpu.get_barrier_semaphore()
    for peer in [pair_t] + [along_z(me_t, k) for k in range(1, n_z)]:
        pl.semaphore_signal(barrier, inc=1, device_id={"tp": peer}, device_id_type=pl.DeviceIdType.MESH)
    for k in range(1, n_dp):
        pl.semaphore_signal(barrier, inc=1, device_id={"dp": dp_peer(k)}, device_id_type=pl.DeviceIdType.MESH)
    pl.semaphore_wait(barrier, n_z + n_dp - 1)

    sends = []

    def remote(src, dst, send, recv, axis, peer):
        return pltpu.make_async_remote_copy(
            src_ref=src, dst_ref=dst, send_sem=send, recv_sem=recv,
            device_id={axis: peer}, device_id_type=pl.DeviceIdType.MESH,
        )

    def start(*args):
        c = remote(*args)
        c.start()
        sends.append(c)

    for b in range(BLOCKS):
        x_src = x_ref if b == 0 else xg.at[b, me_t]

        def pass_on(x_from, g_from, slot, index, peer):
            if b == 0:
                start(g_from, gg.at[slot], g_send.at[index], g_recv.at[slot], "tp", peer)
            start(x_from, xg.at[b, slot], x_send.at[b, index], x_recv.at[b, slot], "tp", peer)

        def arrived(slot):
            if b == 0:
                remote(gain_ref, gg.at[slot], g_send.at[0], g_recv.at[slot], "tp", pair_t).wait_recv()
            remote(x_src, xg.at[b, slot], x_send.at[b, 0], x_recv.at[b, slot], "tp", pair_t).wait_recv()

        def take(slot, x, g, squares):
            xf = x.astype(F32)
            scaled[:, pl.ds(pl.multiple_of(slot * feats, LANES), feats)] = (xf * g).astype(BF16)
            return squares + xf * xf

        for k in range(1, n_z):
            pass_on(x_src, gain_ref, me_t, k, along_z(me_t, k))
        pass_on(x_src, gain_ref, me_t, n_z, pair_t)
        squares = take(me_t, x_src[...], gain_ref[b:b + 1, :], jnp.zeros((batch, feats), F32))
        arrived(pair_t)
        squares = take(pair_t, xg[b, pair_t], gg[pair_t, b:b + 1, :], squares)
        for k in range(1, n_z):
            src = along_z(me_t, -k)
            arrived(src)
            pass_on(xg.at[b, src], gg.at[src], src, n_z + k, pair_t)
            squares = take(src, xg[b, src], gg[src, b:b + 1, :], squares)
        for k in range(1, n_z):
            src = along_z(pair_t, -k)
            arrived(src)
            squares = take(src, xg[b, src], gg[src, b:b + 1, :], squares)
        ss_buf[b] = jnp.broadcast_to(jnp.sum(squares, axis=1, keepdims=True), (batch, LANES)).reshape(n_dp, own, LANES)
        for k in range(1, n_dp):
            start(ss_buf.at[b, dp_peer(k)], ss_recv.at[b, me_d], ss_send.at[b, k], ss_recv_sem.at[b, me_d], "dp", dp_peer(k))

        def between_chips(r):
            for k in [*range(1, n_x), 0]:
                dst = along_x(me_d, k)
                remote(
                    part.at[b, r, dst], pair_recv.at[b, r, k],
                    q_send.at[b, r, k], q_recv.at[b, r, k], "dp", pair_d,
                ).wait_recv()
                if k:
                    both = part[b, r, dst].astype(F32) + pair_recv[b, r, k].astype(F32)
                    mid[b, r, k] = both.astype(BF16)
                    start(
                        mid.at[b, r, k], part_recv.at[b, r, me_d],
                        p_send.at[b, r, k], p_recv.at[b, r, me_d], "dp", dst,
                    )

        for r in range(ROLES):
            loads[b][r].wait()
            p = jnp.dot(scaled[...], w_buf[b, r], preferred_element_type=F32)
            part[b, r] = p.astype(BF16).reshape(n_dp, own, p.shape[1])
            for k in [*range(1, n_x), 0]:
                start(
                    part.at[b, r, along_x(pair_d, k)], pair_recv.at[b, r, k],
                    q_send.at[b, r, k], q_recv.at[b, r, k], "dp", pair_d,
                )
            if r:
                between_chips(r - 1)
        between_chips(ROLES - 1)
        total_sq = ss_buf[b, me_d]
        for k in range(1, n_dp):
            src = lax.rem(me_d - k + n_dp, n_dp)
            remote(ss_buf.at[b, src], ss_recv.at[b, src], ss_send.at[b, k], ss_recv_sem.at[b, src], "dp", src).wait_recv()
            total_sq = total_sq + ss_recv[b, src]
        scale = lax.rsqrt(total_sq / D + norm_eps)[:, 0:1]
        proj = []
        for r in range(ROLES):
            total = part[b, r, me_d].astype(F32) + pair_recv[b, r, 0].astype(F32)
            for k in range(1, n_x):
                src = along_x(me_d, -k)
                remote(
                    mid.at[b, r, k], part_recv.at[b, r, src],
                    p_send.at[b, r, k], p_recv.at[b, r, src], "dp", src,
                ).wait_recv()
                total = total + part_recv[b, r, src].astype(F32)
            proj.append((total * scale).astype(BF16).astype(F32))
        pq, pf, pv, pg = proj
        bound = bound_ref[b:b + 1, :]
        query = silu(pq)
        forget = bound + (1.0 - bound) * sigmoid(pf)
        key = (1.0 - bound) * sigmoid(-pf)
        forget_ref[b] = forget
        value_ref[b] = pv
        coef[...] = query * forget
        qk = query * key
        loads[b][4].wait()

        @pl.loop(0, heads)
        def _(h):
            lanes = pl.ds(pl.multiple_of(h * HEAD_DIM, HEAD_DIM), HEAD_DIM)
            columns = coef[:, lanes].T
            for s in range(own):
                read[pl.ds(s, 1), lanes] = jnp.sum(columns[:, s:s + 1] * s_buf[b, s, h], axis=0, keepdims=True)

        hidden = []
        for h in range(heads):
            lanes = slice(h * HEAD_DIM, (h + 1) * HEAD_DIM)
            row = read[:, lanes] + jnp.sum(qk[:, lanes], axis=1, keepdims=True) * pv[:, lanes]
            normed = row * lax.rsqrt(jnp.mean(row * row, axis=1, keepdims=True) + norm_eps)
            normed = normed * h_gain_ref[b:b + 1, lanes]
            hg[b, me_d, :, lanes] = (normed * silu(pg[:, lanes])).astype(BF16)
        for k in range(1, n_dp):
            start(hg.at[b, me_d], hg.at[b, me_d], h_send.at[b, k], h_recv.at[b, me_d], "dp", dp_peer(k))
        for k in range(1, n_dp):
            src = lax.rem(me_d - k + n_dp, n_dp)
            remote(hg.at[b, src], hg.at[b, src], h_send.at[b, k], h_recv.at[b, src], "dp", src).wait_recv()
        loads[b][5].wait()
        everyone = hg[b].reshape(batch, hg.shape[3])

        def piece(dst):
            lanes = pl.ds(pl.multiple_of(dst * feats, LANES), feats)
            return jnp.dot(everyone, wo_buf[b, :, lanes], preferred_element_type=F32)

        order = [*range(1, n_z), 0]
        for k in order:
            terms[b, k] = piece(along_z(pair_t, k)).astype(BF16)
            start(terms.at[b, k], pair_terms.at[b, k], y_send.at[b, k], y_recv.at[b, k], "tp", pair_t)
        for k in order:
            total = piece(along_z(me_t, k))
            remote(terms.at[b, k], pair_terms.at[b, k], y_send.at[b, k], y_recv.at[b, k], "tp", pair_t).wait_recv()
            total = total + pair_terms[b, k].astype(F32)
            if k:
                mid_terms[b, k] = total.astype(BF16)
                start(
                    mid_terms.at[b, k], terms_recv.at[b, me_t], t_send.at[b, k], t_recv.at[b, me_t],
                    "tp", along_z(me_t, k),
                )
        for k in range(1, n_z):
            src = along_z(me_t, -k)
            remote(mid_terms.at[b, k], terms_recv.at[b, src], t_send.at[b, k], t_recv.at[b, src], "tp", src).wait_recv()
            total = total + terms_recv[b, src].astype(F32)
        x_next = (x_src[...].astype(F32) + total).astype(BF16)
        if b + 1 < BLOCKS:
            xg[b + 1, me_t] = x_next
        else:
            out_ref[...] = x_next
    for c in sends:
        c.wait_send()


def update_kernel(forget_ref, value_ref, state_ref, new_ref):
    rows, heads = state_ref.shape[1], state_ref.shape[2]
    for h in range(heads):
        lanes = slice(h * HEAD_DIM, (h + 1) * HEAD_DIM)
        f = forget_ref[0, :, lanes].T
        for s in range(rows):
            v = value_ref[0, s:s + 1, lanes]
            new_ref[0, s, h] = v + f[:, s:s + 1] * (state_ref[0, s, h] - v)


def fast_body(
    n_tp, n_dp, residual, norm_gain, w_query, w_forget, w_value, w_output_gate, lower_bound, head_gain, w_out, state
):
    batch, feats = residual.shape
    rows, cols = w_query.shape[1:]
    own, heads = state.shape[1:3]
    gain = jnp.pad(norm_gain.astype(F32), ((0, 8 - BLOCKS), (0, 0)))
    vmem = pl.BlockSpec(memory_space=pltpu.VMEM)
    hbm = pl.BlockSpec(memory_space=pl.ANY)
    small = jax.ShapeDtypeStruct((BLOCKS, own, cols), F32)
    dma = pltpu.SemaphoreType.DMA
    new_residual, forget, value = pl.pallas_call(
        functools.partial(step_kernel, n_tp, n_dp),
        out_shape=(jax.ShapeDtypeStruct((batch, feats), BF16), small, small),
        in_specs=[vmem] * 4 + [hbm] * 6,
        out_specs=(vmem,) * 3,
        scratch_shapes=[
            pltpu.VMEM((BLOCKS, ROLES, rows, cols), BF16),
            pltpu.VMEM((BLOCKS, *w_out.shape[1:]), BF16),
            pltpu.VMEM(state.shape, F32),
            pltpu.VMEM((BLOCKS, n_tp, batch, feats), BF16),
            pltpu.VMEM((n_tp, 8, feats), F32),
            pltpu.VMEM((batch, rows), BF16),
            pltpu.VMEM((BLOCKS, n_dp, own, LANES), F32),
            pltpu.VMEM((BLOCKS, n_dp, own, LANES), F32),
            pltpu.VMEM((BLOCKS, ROLES, n_dp, own, cols), BF16),
            pltpu.VMEM((BLOCKS, ROLES, n_dp // 2, own, cols), BF16),
            pltpu.VMEM((BLOCKS, ROLES, n_dp // 2, own, cols), BF16),
            pltpu.VMEM((BLOCKS, ROLES, n_dp, own, cols), BF16),
            pltpu.VMEM((own, cols), F32),
            pltpu.VMEM((own, cols), F32),
            pltpu.VMEM((BLOCKS, n_dp, own, cols), BF16),
            pltpu.VMEM((BLOCKS, n_tp // 2, batch, feats), BF16),
            pltpu.VMEM((BLOCKS, n_tp // 2, batch, feats), BF16),
            pltpu.VMEM((BLOCKS, n_tp // 2, batch, feats), BF16),
            pltpu.VMEM((BLOCKS, n_tp, batch, feats), BF16),
            dma((BLOCKS, 6)),
            dma((BLOCKS, n_tp)), dma((BLOCKS, n_tp)),
            dma((n_tp,)), dma((n_tp,)),
            dma((BLOCKS, n_dp)), dma((BLOCKS, n_dp)),
            dma((BLOCKS, ROLES, n_dp // 2)), dma((BLOCKS, ROLES, n_dp // 2)),
            dma((BLOCKS, ROLES, n_dp)), dma((BLOCKS, ROLES, n_dp)),
            dma((BLOCKS, n_dp)), dma((BLOCKS, n_dp)),
            dma((BLOCKS, n_tp // 2)), dma((BLOCKS, n_tp // 2)),
            dma((BLOCKS, n_tp)), dma((BLOCKS, n_tp)),
        ],
        compiler_params=pltpu.CompilerParams(
            collective_id=0, has_side_effects=True, vmem_limit_bytes=56 * 1024 * 1024
        ),
        name="recurrent_step",
    )(
        residual, gain, lower_bound, head_gain.astype(F32),
        w_query, w_forget, w_value, w_output_gate, w_out, state,
    )
    step = 8
    part = pl.BlockSpec((1, step, cols), lambda b, s: (b, s, 0))
    whole = pl.BlockSpec((1, step, heads, HEAD_DIM, HEAD_DIM), lambda b, s: (b, s, 0, 0, 0))
    new_state = pl.pallas_call(
        update_kernel,
        grid=(BLOCKS, own // step),
        out_shape=jax.ShapeDtypeStruct(state.shape, F32),
        in_specs=[part, part, whole],
        out_specs=whole,
        name="state_update",
    )(forget, value, state)
    return new_residual, new_state


def solution(mesh):
    placed = (
        P(None, ("dp", "tp")),
        P(None, ("dp", "tp")),
        P(None, "dp", "tp"),
        P(None, "dp", "tp"),
        P(None, "dp", "tp"),
        P(None, "dp", "tp"),
        P(None, "tp"),
        P(None, "tp"),
        P(None, "tp", "dp"),
        P(None, "dp", "tp", None, None),
    )
    n_tp, n_dp = mesh.shape["tp"], mesh.shape["dp"]
    whole_tiles = D % (n_tp * n_dp * LANES) == 0 and n_tp % 2 == 0 and n_dp % 2 == 0
    return jax.shard_map(
        functools.partial(fast_body, n_tp, n_dp) if whole_tiles else body,
        mesh=mesh,
        in_specs=placed,
        out_specs=(P(None, ("dp", "tp")), P(None, "dp", "tp", None, None)),
        check_vma=False,
    )
```

profile of v0, /device:TPU:0, one launch (start us, length us, event | category | flops | bytes accessed | tf_op | source)
XLA Modules:
  0.0 85.2 jit_solution(7010047288880203455)
XLA Ops:
  0.6 1.3 %pad_convert_fusion.gain_ref = f32[8,128]{1,0:T(8,128)} fusion(bf16[2,128]{1,0:T(2,128)(2,1)} %param.11), kind=kLoop, calls=%fused_computation | loop fusion | flops 1024 | bytes 4608 | tf_op jit(solution)/shard_map/jit(_pad)/pad | solution.py:337
  1.9 1.3 %convert_element_type.6.h_gain_ref = f32[2,512]{1,0:T(2,128)} convert(bf16[2,512]{1,0:T(2,128)(2,1)} %param.17) | non-fusion elementwise | flops 1024 | bytes 6144 | tf_op jit(solution)/shard_map/convert_element_type | solution.py:382
  3.2 65.1 %recurrent_step.1 = (bf16[128,128]{1,0:T(8,128)(2,1)}, f32[2,32,512]{2,1,0:T(8,128)}, f32[2,32,512]{2,1,0:T(8,128)}) custom-call(bf16[128,128]{1,0:T(8,128)(2,1)} %x_ref.1, f32[8,128]{1,0:T(8,128)} %pad_convert_fusion.gain_ref, f32[2,512]{1,0:T(2,128)} %bound_ref.1, f32[2,512]{1,0:T(2,128)} %convert_element_type.6.h_gain_ref, bf16[2,1024,512]{2,1,0:T(8,128)(2,1)} %wq_hbm.1, ...), custom_call_target="tpu_custom_call" | custom-call | tf_op jit(solution)/shard_map/recurrent_step/pallas_call | solution.py:342
  68.2 0.0 copy-start
  68.2 16.4 %state_update.1 = f32[2,32,4,128,128]{4,3,2,1,0:T(8,128)} custom-call(f32[2,32,512]{2,1,0:T(8,128)} %get-tuple-element.6.forget_ref, f32[2,32,512]{2,1,0:T(8,128)} %get-tuple-element.7.value_ref, f32[2,32,4,128,128]{4,3,2,1,0:T(8,128)} %state_ref.1), custom_call_target="tpu_custom_call" | custom-call | tf_op jit(solution)/shard_map/state_update/pallas_call | solution.py:388
  84.6 0.0 copy-done
  84.6 0.6 copy.13
Async XLA Ops:
  68.2 16.4 %copy-start = (bf16[128,128]{1,0:T(8,128)(2,1)S(1)}, bf16[128,128]{1,0:T(8,128)(2,1)}, u32[]{:S(2)}) copy-start(bf16[128,128]{1,0:T(8,128)(2,1)} %get-tuple-element.10) | copy-start | bytes 98308
where the time goes:
time: 85.5 us; the launch traced here: 85.2 us
  Pallas kernels  81.4 us (95%)
  other arithmetic  2.53 us (3%)
    pallas_call x1, Pallas kernels, fast_body(): pl.pallas_call(functools.partial(step_kernel, n_tp, n_dp), out_shape=(jax...  65.1 us
    pallas_call x1, Pallas kernels, fast_body(): pl.pallas_call(update_kernel, grid=(BLOCKS, own // step), out_shape=jax.S...  16.4 us

commit v1 on v0

--- a/solution.py
+++ b/solution.py
@@ -102,6 +102,7 @@
 
 LANES = 128
 ROLES = 4
+PIECES = 8
 F32 = jnp.float32
 BF16 = jnp.bfloat16
 
@@ -116,11 +117,11 @@
 
 def step_kernel(
     n_tp, n_dp,
-    x_ref, gain_ref, bound_ref, h_gain_ref, wq_hbm, wf_hbm, wv_hbm, wg_hbm, wo_hbm, state_hbm,
-    out_ref, forget_ref, value_ref,
-    w_buf, wo_buf, s_buf, xg, gg, scaled, ss_buf, ss_recv, part, pair_recv, mid, part_recv, coef, read, hg,
+    x_hbm, gain_hbm, bound_hbm, h_gain_hbm, wq_hbm, wf_hbm, wv_hbm, wg_hbm, wo_hbm, state_hbm,
+    out_ref, s_buf,
+    x_ref, raw_gain_ref, bound_ref, raw_h_gain_ref, gain_ref, forget_ref, value_ref, w_buf, wo_buf, xg, gg, scaled, ss_buf, ss_recv, part, pair_recv, mid, part_recv, coef, read, hg,
     terms, pair_terms, mid_terms, terms_recv,
-    load_sem, x_send, x_recv, g_send, g_recv, ss_send, ss_recv_sem, q_send, q_recv, p_send, p_recv,
+    small_sem, load_sem, x_send, x_recv, g_send, g_recv, ss_send, ss_recv_sem, q_send, q_recv, p_send, p_recv,
     h_send, h_recv, y_send, y_recv, t_send, t_recv,
 ):
     me_t, me_d = lax.axis_index("tp"), lax.axis_index("dp")
@@ -141,6 +142,14 @@
     def dp_peer(k):
         return lax.rem(me_d + k, n_dp)
 
+    small = [
+        pltpu.make_async_copy(src, dst, small_sem.at[i])
+        for i, (src, dst) in enumerate((
+            (x_hbm, x_ref), (gain_hbm, raw_gain_ref), (bound_hbm, bound_ref), (h_gain_hbm, raw_h_gain_ref),
+        ))
+    ]
+    for c in small:
+        c.start()
     loads = []
     for b in range(BLOCKS):
         group = [
@@ -160,7 +169,18 @@
         pl.semaphore_signal(barrier, inc=1, device_id={"dp": dp_peer(k)}, device_id_type=pl.DeviceIdType.MESH)
     pl.semaphore_wait(barrier, n_z + n_dp - 1)
 
+    for c in small:
+        c.wait()
+    gain_ref[pl.ds(0, BLOCKS), :] = raw_gain_ref[...].astype(F32)
+    h_gain = raw_h_gain_ref[...].astype(F32)
     sends = []
+
+    def update(b, h):
+        lanes = slice(h * HEAD_DIM, (h + 1) * HEAD_DIM)
+        f = forget_ref[b, :, lanes].T
+        for s in range(own):
+            v = value_ref[b, s:s + 1, lanes]
+            s_buf[b, s, h] = v + f[:, s:s + 1] * (s_buf[b, s, h] - v)
 
     def remote(src, dst, send, recv, axis, peer):
         return pltpu.make_async_remote_copy(
@@ -277,10 +297,12 @@
             lanes = slice(h * HEAD_DIM, (h + 1) * HEAD_DIM)
             row = read[:, lanes] + jnp.sum(qk[:, lanes], axis=1, keepdims=True) * pv[:, lanes]
             normed = row * lax.rsqrt(jnp.mean(row * row, axis=1, keepdims=True) + norm_eps)
-            normed = normed * h_gain_ref[b:b + 1, lanes]
+            normed = normed * h_gain[b:b + 1, lanes]
             hg[b, me_d, :, lanes] = (normed * silu(pg[:, lanes])).astype(BF16)
         for k in range(1, n_dp):
             start(hg.at[b, me_d], hg.at[b, me_d], h_send.at[b, k], h_recv.at[b, me_d], "dp", dp_peer(k))
+        for h in range(heads // 2):
+            update(b, h)
         for k in range(1, n_dp):
             src = lax.rem(me_d - k + n_dp, n_dp)
             remote(hg.at[b, src], hg.at[b, src], h_send.at[b, k], h_recv.at[b, src], "dp", src).wait_recv()
@@ -295,6 +317,8 @@
         for k in order:
             terms[b, k] = piece(along_z(pair_t, k)).astype(BF16)
             start(terms.at[b, k], pair_terms.at[b, k], y_send.at[b, k], y_recv.at[b, k], "tp", pair_t)
+        for h in range(heads // 2, heads):
+            update(b, h)
         for k in order:
             total = piece(along_z(me_t, k))
             remote(terms.at[b, k], pair_terms.at[b, k], y_send.at[b, k], y_recv.at[b, k], "tp", pair_t).wait_recv()
@@ -318,14 +342,17 @@
         c.wait_send()
 
 
-def update_kernel(forget_ref, value_ref, state_ref, new_ref):
-    rows, heads = state_ref.shape[1], state_ref.shape[2]
-    for h in range(heads):
-        lanes = slice(h * HEAD_DIM, (h + 1) * HEAD_DIM)
-        f = forget_ref[0, :, lanes].T
-        for s in range(rows):
-            v = value_ref[0, s:s + 1, lanes]
-            new_ref[0, s, h] = v + f[:, s:s + 1] * (state_ref[0, s, h] - v)
+def flush_kernel(x_ref, state_ref, out_ref, new_ref, sem):
+    blocks, rows = state_ref.shape[:2]
+    copies = [pltpu.make_async_copy(x_ref, out_ref, sem.at[0, 0])]
+    for b in range(blocks):
+        for c in range(PIECES):
+            part = pl.ds(c * (rows // PIECES), rows // PIECES)
+            copies.append(pltpu.make_async_copy(state_ref.at[b, part], new_ref.at[b, part], sem.at[1 + b, c]))
+    for c in copies:
+        c.start()
+    for c in copies:
+        c.wait()
 
 
 def fast_body(
@@ -334,20 +361,24 @@
     batch, feats = residual.shape
     rows, cols = w_query.shape[1:]
     own, heads = state.shape[1:3]
-    gain = jnp.pad(norm_gain.astype(F32), ((0, 8 - BLOCKS), (0, 0)))
     vmem = pl.BlockSpec(memory_space=pltpu.VMEM)
-    hbm = pl.BlockSpec(memory_space=pl.ANY)
-    small = jax.ShapeDtypeStruct((BLOCKS, own, cols), F32)
+    hbm = pl.BlockSpec(memory_space=pltpu.HBM)
     dma = pltpu.SemaphoreType.DMA
-    new_residual, forget, value = pl.pallas_call(
+    current, fresh = pl.pallas_call(
         functools.partial(step_kernel, n_tp, n_dp),
-        out_shape=(jax.ShapeDtypeStruct((batch, feats), BF16), small, small),
-        in_specs=[vmem] * 4 + [hbm] * 6,
-        out_specs=(vmem,) * 3,
+        out_shape=(pltpu.VMEM((batch, feats), BF16), pltpu.VMEM(state.shape, F32)),
+        in_specs=[hbm] * 10,
+        out_specs=(vmem,) * 2,
         scratch_shapes=[
+            pltpu.VMEM((batch, feats), BF16),
+            pltpu.VMEM(norm_gain.shape, norm_gain.dtype),
+            pltpu.VMEM(lower_bound.shape, lower_bound.dtype),
+            pltpu.VMEM(head_gain.shape, head_gain.dtype),
+            pltpu.VMEM((8, feats), F32),
+            pltpu.VMEM((BLOCKS, own, cols), F32),
+            pltpu.VMEM((BLOCKS, own, cols), F32),
             pltpu.VMEM((BLOCKS, ROLES, rows, cols), BF16),
             pltpu.VMEM((BLOCKS, *w_out.shape[1:]), BF16),
-            pltpu.VMEM(state.shape, F32),
             pltpu.VMEM((BLOCKS, n_tp, batch, feats), BF16),
             pltpu.VMEM((n_tp, 8, feats), F32),
             pltpu.VMEM((batch, rows), BF16),
@@ -364,6 +395,7 @@
             pltpu.VMEM((BLOCKS, n_tp // 2, batch, feats), BF16),
             pltpu.VMEM((BLOCKS, n_tp // 2, batch, feats), BF16),
             pltpu.VMEM((BLOCKS, n_tp, batch, feats), BF16),
+            dma((4,)),
             dma((BLOCKS, 6)),
             dma((BLOCKS, n_tp)), dma((BLOCKS, n_tp)),
             dma((n_tp,)), dma((n_tp,)),
@@ -375,25 +407,29 @@
             dma((BLOCKS, n_tp)), dma((BLOCKS, n_tp)),
         ],
         compiler_params=pltpu.CompilerParams(
-            collective_id=0, has_side_effects=True, vmem_limit_bytes=56 * 1024 * 1024
+            collective_id=0, has_side_effects=True, vmem_limit_bytes=32 * 1024 * 1024
         ),
         name="recurrent_step",
     )(
-        residual, gain, lower_bound, head_gain.astype(F32),
-        w_query, w_forget, w_value, w_output_gate, w_out, state,
-    )
-    step = 8
-    part = pl.BlockSpec((1, step, cols), lambda b, s: (b, s, 0))
-    whole = pl.BlockSpec((1, step, heads, HEAD_DIM, HEAD_DIM), lambda b, s: (b, s, 0, 0, 0))
-    new_state = pl.pallas_call(
-        update_kernel,
-        grid=(BLOCKS, own // step),
-        out_shape=jax.ShapeDtypeStruct(state.shape, F32),
-        in_specs=[part, part, whole],
-        out_specs=whole,
-        name="state_update",
-    )(forget, value, state)
-    return new_residual, new_state
+        *(
+            pltpu.with_memory_space_constraint(a, pltpu.HBM)
+            for a in (
+                residual, norm_gain, lower_bound, head_gain, w_query, w_forget, w_value, w_output_gate, w_out, state
+            )
+        )
+    )
+    return tuple(pl.pallas_call(
+        flush_kernel,
+        out_shape=(jax.ShapeDtypeStruct((batch, feats), BF16), jax.ShapeDtypeStruct(state.shape, F32)),
+        in_specs=[vmem] * 2,
+        out_specs=(hbm,) * 2,
+        scratch_shapes=[dma((1 + BLOCKS, PIECES))],
+        compiler_params=pltpu.CompilerParams(vmem_limit_bytes=4 * 1024 * 1024),
+        name="flush",
+    )(
+        pltpu.with_memory_space_constraint(current, pltpu.VMEM),
+        pltpu.with_memory_space_constraint(fresh, pltpu.VMEM),
+    ))
 
 
 def solution(mesh):

time: 85.5 us -> 76.9 us (0.90)
  Pallas kernels: 81.4 us -> 76.1 us
  other arithmetic: 2.53 us -> 0 us
    pallas_call x2, Pallas kernels: 81.4 us -> 76.1 us  [the longest x1 70 us: fast_body(): pl.pallas_call(functools.partial(step_kernel, n_tp, n_dp), out_shape=(plt...]
    convert_element_type x1 -> x0, other arithmetic: 1.28 us -> none  [fast_body(): head_gain.astype(F32)]
    pad x1 -> x0, other arithmetic: 1.25 us -> none  [fast_body(): gain = jnp.pad(norm_gain.astype(F32), ((0, 8 - BLOCKS), (0, 0)))]
where the time goes in v1:
time: 76.9 us; the launch traced here: 76.7 us
  Pallas kernels  76.1 us (99%)
    pallas_call x1, Pallas kernels, fast_body(): pl.pallas_call(functools.partial(step_kernel, n_tp, n_dp), out_shape=(plt...  70 us
    pallas_call x1, Pallas kernels, fast_body(): pl.pallas_call(flush_kernel, out_shape=(jax.ShapeDtypeStruct((batch, feat...  6.04 us

profile of v1, /device:TPU:0, one launch (start us, length us, event | category | flops | bytes accessed | tf_op | source)
XLA Modules:
  0.0 76.7 jit_solution(114480284321352310)
XLA Ops:
  0.6 70.0 %recurrent_step.1 = (bf16[128,128]{1,0:T(8,128)(2,1)S(1)}, f32[2,32,4,128,128]{4,3,2,1,0:T(8,128)S(1)}) custom-call(bf16[128,128]{1,0:T(8,128)(2,1)} %x_hbm.1, bf16[2,128]{1,0:T(2,128)(2,1)} %gain_hbm.1, f32[2,512]{1,0:T(2,128)} %bound_hbm.1, bf16[2,512]{1,0:T(2,128)(2,1)} %h_gain_hbm.1, bf16[2,1024,512]{2,1,0:T(8,128)(2,1)} %wq_hbm.1, ...), custom_call_target="tpu_custom_call" | custom-call | tf_op jit(solution)/shard_map/recurrent_step/pallas_call | solution.py:367
  70.7 6.0 %flush.1 = (bf16[128,128]{1,0:T(8,128)(2,1)}, f32[2,32,4,128,128]{4,3,2,1,0:T(8,128)}) custom-call(bf16[128,128]{1,0:T(8,128)(2,1)S(1)} %get-tuple-element.4.x_ref, f32[2,32,4,128,128]{4,3,2,1,0:T(8,128)S(1)} %get-tuple-element.5.state_ref), custom_call_target="tpu_custom_call" | custom-call | tf_op jit(solution)/shard_map/flush/pallas_call | solution.py:421

commit v2 on v1

v2 whole, which is shorter than its diff:
```python
import functools

import jax
import jax.numpy as jnp
from jax import lax
from jax.experimental import pallas as pl
from jax.experimental.pallas import tpu as pltpu
from jax.sharding import PartitionSpec as P

D = 4096
HEAD_DIM = 128
BLOCKS = 2


norm_eps = 1e-06


def one_block(x, gain, w_q, w_f, w_v, w_g, bound, h_gain, w_o, old_state):
    xf = x.astype(jnp.float32)
    x_whole, g_whole = (
        lax.all_gather(x, "tp", axis=1, tiled=True),
        lax.all_gather(gain, "tp", axis=1, tiled=True),
    )
    x_wide = x_whole.astype(jnp.float32)
    scaled = (x_wide * g_whole.astype(jnp.float32)).astype(jnp.bfloat16)
    part_q = jnp.dot(scaled, w_q, preferred_element_type=jnp.float32)
    part_f = jnp.dot(scaled, w_f, preferred_element_type=jnp.float32)
    part_v = jnp.dot(scaled, w_v, preferred_element_type=jnp.float32)
    part_g = jnp.dot(scaled, w_g, preferred_element_type=jnp.float32)
    total_sq = lax.psum(jnp.sum(x_wide * x_wide, axis=1), "dp")
    pq, pf, pv, pg = (
        lax.psum_scatter(part_q.astype(jnp.bfloat16), "dp", scatter_dimension=0, tiled=True).astype(
            jnp.float32
        ),
        lax.psum_scatter(part_f.astype(jnp.bfloat16), "dp", scatter_dimension=0, tiled=True).astype(
            jnp.float32
        ),
        lax.psum_scatter(part_v.astype(jnp.bfloat16), "dp", scatter_dimension=0, tiled=True).astype(
            jnp.float32
        ),
        lax.psum_scatter(part_g.astype(jnp.bfloat16), "dp", scatter_dimension=0, tiled=True).astype(
            jnp.float32
        ),
    )
    own = pq.shape[0]
    own_sq = lax.dynamic_slice_in_dim(total_sq, lax.axis_index("dp") * own, own, 0)
    scale = lax.rsqrt(own_sq / D + norm_eps)[:, None]

    def finish(total):
        return lax.optimization_barrier((total * scale).astype(jnp.bfloat16)).astype(jnp.float32)

    pq, pf, pv, pg = (finish(pq), finish(pf), finish(pv), finish(pg))
    heads_here = old_state.shape[1]
    query = jax.nn.silu(pq).reshape(own, heads_here, HEAD_DIM)
    forget = (bound + (1.0 - bound) * jax.nn.sigmoid(pf)).reshape(own, heads_here, HEAD_DIM)
    key = ((1.0 - bound) * jax.nn.sigmoid(-pf)).reshape(own, heads_here, HEAD_DIM)
    value = pv.reshape(own, heads_here, HEAD_DIM)
    fresh = forget[..., None] * old_state + key[..., None] * value[:, :, None, :]
    read = jnp.einsum("bhk,bhkv->bhv", query, fresh)
    normed = read * lax.rsqrt(jnp.mean(read * read, axis=2, keepdims=True) + norm_eps)
    normed = normed.reshape(own, heads_here * HEAD_DIM) * h_gain.astype(jnp.float32)
    hidden = (normed * jax.nn.silu(pg)).astype(jnp.bfloat16)
    terms = jnp.dot(
        lax.all_gather(hidden, "dp", axis=0, tiled=True), w_o, preferred_element_type=jnp.float32
    )
    mixed = lax.psum_scatter(
        terms.astype(jnp.bfloat16), "tp", scatter_dimension=1, tiled=True
    ).astype(jnp.float32)
    return ((xf + mixed).astype(jnp.bfloat16), fresh)


def body(
    residual,
    norm_gain,
    w_query,
    w_forget,
    w_value,
    w_output_gate,
    lower_bound,
    head_gain,
    w_out,
    state,
):
    current = residual
    states = []
    for layer in range(BLOCKS):
        current, fresh = one_block(
            current,
            norm_gain[layer : layer + 1],
            w_query[layer],
            w_forget[layer],
            w_value[layer],
            w_output_gate[layer],
            lower_bound[layer],
            head_gain[layer],
            w_out[layer],
            state[layer],
        )
        states.append(fresh)
    return (current, jnp.stack(states))


LANES = 128
ROLES = 4
PIECES = 8
HALVES = 2
F32 = jnp.float32
BF16 = jnp.bfloat16


def silu(v):
    return v / (1.0 + jnp.exp(-v))


def sigmoid(v):
    return 1.0 / (1.0 + jnp.exp(-v))


def flip(v, bit):
    return v + bit * (1 - 2 * lax.rem(lax.div(v, bit), 2))


def ranked(z, n_z):
    if n_z == 4:
        upper = lax.div(z, 2)
        return [3 - 3 * upper, 2 - upper, flip(z, 1)]
    others = []
    for k in range(n_z - 1, 0, -1):
        other, bit = z, 1
        while bit <= k:
            other = flip(other, bit) if k & bit else other
            bit *= 2
        others.append(other)
    return others


def step_kernel(
    n_tp, n_dp,
    x_hbm, gain_hbm, bound_hbm, h_gain_hbm, wq_hbm, wf_hbm, wv_hbm, wg_hbm, wo_hbm, state_hbm,
    out_ref, s_buf,
    raw_gain_ref, bound_ref, raw_h_gain_ref, gain_ref, forget_ref, value_ref, w_buf, wo_buf, xg, gg, scaled, sq,
    ss_buf, ss_recv, part, pair_recv, mid, part_recv, coef, read, hg, acc, terms, pair_terms, mid_terms, terms_recv,
    small_sem, load_sem, x_send, x_recv, g_send, g_recv, ss_send, ss_recv_sem, q_send, q_recv, p_send, p_recv,
    h_send, h_recv, y_send, y_recv, t_send, t_recv,
):
    me_t, me_d = lax.axis_index("tp"), lax.axis_index("dp")
    batch, feats = x_hbm.shape
    own, heads = s_buf.shape[1:3]
    rows, cols = w_buf.shape[2:]
    half, many = own // HALVES, batch // HALVES

    n_z, n_x = n_tp // 2, n_dp // 2
    me_y, me_z = lax.rem(me_t, 2), lax.div(me_t, 2)
    pair_t, pair_d = flip(me_t, 1), flip(me_d, 1)
    peers = ranked(me_z, n_z)
    near_first = [*reversed([*enumerate(peers)])]

    def along_x(d, k):
        return lax.rem(d + 2 * k + n_dp, n_dp)

    def dp_peer(k):
        return lax.rem(me_d + k, n_dp)

    def columns_of(slot):
        return pl.ds(pl.multiple_of(slot * feats, LANES), feats)

    small = []
    for h in range(HALVES):
        for d in range(n_dp):
            small.append((x_hbm.at[pl.ds(d * own + h * half, half)], xg.at[0, h, me_t, pl.ds(d * half, half)]))
    small += [(gain_hbm, raw_gain_ref), (bound_hbm, bound_ref), (h_gain_hbm, raw_h_gain_ref)]
    small = [pltpu.make_async_copy(src, dst, small_sem.at[i]) for i, (src, dst) in enumerate(small)]
    for c in small:
        c.start()

    barrier = pltpu.get_barrier_semaphore()
    for peer in [pair_t] + [2 * z + me_y for z in peers]:
        pl.semaphore_signal(barrier, inc=1, device_id={"tp": peer}, device_id_type=pl.DeviceIdType.MESH)
    for k in range(1, n_dp):
        pl.semaphore_signal(barrier, inc=1, device_id={"dp": dp_peer(k)}, device_id_type=pl.DeviceIdType.MESH)
    for c in small:
        c.wait()
    gain_ref[pl.ds(0, BLOCKS), :] = raw_gain_ref[...].astype(F32)
    h_gain = raw_h_gain_ref[...].astype(F32)

    loads = []
    for b in range(BLOCKS):
        group = [
            pltpu.make_async_copy(w.at[b], w_buf.at[b, r], load_sem.at[b, r])
            for r, w in enumerate((wq_hbm, wf_hbm, wv_hbm, wg_hbm))
        ]
        group.append(pltpu.make_async_copy(state_hbm.at[b], s_buf.at[b], load_sem.at[b, ROLES]))
        group.append(pltpu.make_async_copy(wo_hbm.at[b], wo_buf.at[b], load_sem.at[b, ROLES + 1]))
        loads.append(group)
    for c in loads[0][:ROLES]:
        c.start()
    pl.semaphore_wait(barrier, n_z + n_dp - 1)

    sends = []

    def remote(src, dst, send, recv, axis, peer):
        return pltpu.make_async_remote_copy(
            src_ref=src, dst_ref=dst, send_sem=send, recv_sem=recv,
            device_id={axis: peer}, device_id_type=pl.DeviceIdType.MESH,
        )

    def start(*args):
        c = remote(*args)
        c.start()
        sends.append(c)

    def pass_on(b, h, slot, index, peer):
        if b == 0 and h == 0:
            start(gain_ref if slot is me_t else gg.at[slot], gg.at[slot], g_send.at[index], g_recv.at[slot], "tp", peer)
        block = xg.at[b, h, slot]
        start(block, block, x_send.at[b, h, index], x_recv.at[b, h, slot], "tp", peer)

    def arrived(b, h, slot):
        if b == 0 and h == 0:
            remote(gg.at[slot], gg.at[slot], g_send.at[0], g_recv.at[slot], "tp", pair_t).wait_recv()
        block = xg.at[b, h, slot]
        remote(block, block, x_send.at[b, h, 0], x_recv.at[b, h, slot], "tp", pair_t).wait_recv()

    def take(b, h, slot):
        xf = xg[b, h, slot].astype(F32)
        g = (gain_ref if slot is me_t else gg.at[slot])[b:b + 1, :]
        scaled[h, :, columns_of(slot)] = (xf * g).astype(BF16)
        sq[h] = xf * xf if slot is me_t else sq[h] + xf * xf

    def gather_send(b, h):
        for j, z in enumerate(peers):
            pass_on(b, h, me_t, j, 2 * z + me_y)
        pass_on(b, h, me_t, n_z - 1, pair_t)
        take(b, h, me_t)

    def gather_along_z(b, h):
        for j, z in near_first:
            slot = 2 * z + me_y
            arrived(b, h, slot)
            pass_on(b, h, slot, n_z + j, pair_t)
            take(b, h, slot)

    def gather_along_y(b, h):
        for slot in [pair_t] + [2 * z + 1 - me_y for _, z in near_first]:
            arrived(b, h, slot)
            take(b, h, slot)
        total = jnp.sum(sq[h], axis=1, keepdims=True)
        ss_buf[b, h] = jnp.broadcast_to(total, (many, LANES)).reshape(n_dp, half, LANES)
        for k in range(1, n_dp):
            start(
                ss_buf.at[b, h, dp_peer(k)], ss_recv.at[b, h, me_d],
                ss_send.at[b, h, k], ss_recv_sem.at[b, h, me_d], "dp", dp_peer(k),
            )

    def project(b, h, r):
        if h == 0:
            loads[b][r].wait()
        p = jnp.dot(scaled[h], w_buf[b, r], preferred_element_type=F32)
        part[b, h, r] = p.astype(BF16).reshape(n_dp, half, cols)
        for k in [*range(1, n_x), 0]:
            start(
                part.at[b, h, r, along_x(pair_d, k)], pair_recv.at[b, h, r, k],
                q_send.at[b, h, r, k], q_recv.at[b, h, r, k], "dp", pair_d,
            )

    def between_chips(b, h, r):
        for k in [*range(1, n_x), 0]:
            dst = along_x(me_d, k)
            remote(
                part.at[b, h, r, dst], pair_recv.at[b, h, r, k],
                q_send.at[b, h, r, k], q_recv.at[b, h, r, k], "dp", pair_d,
            ).wait_recv()
            if k:
                both = part[b, h, r, dst].astype(F32) + pair_recv[b, h, r, k].astype(F32)
                mid[b, h, r, k] = both.astype(BF16)
                start(
                    mid.at[b, h, r, k], part_recv.at[b, h, r, me_d],
                    p_send.at[b, h, r, k], p_recv.at[b, h, r, me_d], "dp", dst,
                )

    def read_out(b, h):
        total_sq = ss_buf[b, h, me_d]
        for k in range(1, n_dp):
            src = lax.rem(me_d - k + n_dp, n_dp)
            remote(
                ss_buf.at[b, h, src], ss_recv.at[b, h, src],
                ss_send.at[b, h, k], ss_recv_sem.at[b, h, src], "dp", src,
            ).wait_recv()
            total_sq = total_sq + ss_recv[b, h, src]
        scale = lax.rsqrt(total_sq / (rows * n_dp) + norm_eps)[:, 0:1]
        proj = []
        for r in range(ROLES):
            total = part[b, h, r, me_d].astype(F32) + pair_recv[b, h, r, 0].astype(F32)
            for k in range(1, n_x):
                src = along_x(me_d, -k)
                remote(
                    mid.at[b, h, r, k], part_recv.at[b, h, r, src],
                    p_send.at[b, h, r, k], p_recv.at[b, h, r, src], "dp", src,
                ).wait_recv()
                total = total + part_recv[b, h, r, src].astype(F32)
            proj.append((total * scale).astype(BF16).astype(F32))
        pq, pf, pv, pg = proj
        bound = bound_ref[b:b + 1, :]
        query = silu(pq)
        forget = bound + (1.0 - bound) * sigmoid(pf)
        key = (1.0 - bound) * sigmoid(-pf)
        forget_ref[b, h] = forget
        value_ref[b, h] = pv
        coef[h] = query * forget
        qk = query * key
        if h == 0:
            loads[b][ROLES].wait()

        @pl.loop(0, heads)
        def _(head):
            lanes = pl.ds(pl.multiple_of(head * HEAD_DIM, HEAD_DIM), HEAD_DIM)
            factors = coef[h, :, lanes]
            for s in range(half):
                sums = jnp.dot(factors, s_buf[b, h * half + s, head], preferred_element_type=F32)
                read[h, pl.ds(s, 1), lanes] = sums[s:s + 1]

        for head in range(heads):
            lanes = slice(head * HEAD_DIM, (head + 1) * HEAD_DIM)
            row = read[h, :, lanes] + jnp.sum(qk[:, lanes], axis=1, keepdims=True) * pv[:, lanes]
            normed = row * lax.rsqrt(jnp.mean(row * row, axis=1, keepdims=True) + norm_eps)
            normed = normed * h_gain[b:b + 1, lanes]
            hg[b, h, me_d, :, lanes] = (normed * silu(pg[:, lanes])).astype(BF16)
        for k in range(1, n_dp):
            mine = hg.at[b, h, me_d]
            start(mine, mine, h_send.at[b, h, k], h_recv.at[b, h, me_d], "dp", dp_peer(k))

    def mix(b, h):
        for k in range(1, n_dp):
            src = lax.rem(me_d - k + n_dp, n_dp)
            theirs = hg.at[b, h, src]
            remote(theirs, theirs, h_send.at[b, h, k], h_recv.at[b, h, src], "dp", src).wait_recv()
        if h == 0:
            loads[b][ROLES + 1].wait()
        everyone = hg[b, h].reshape(many, cols)
        acc[h] = jnp.dot(everyone, wo_buf[b], preferred_element_type=F32)
        for j, z in enumerate([*peers, me_z]):
            terms[b, h, j] = acc[h, :, columns_of(2 * z + 1 - me_y)].astype(BF16)
            start(terms.at[b, h, j], pair_terms.at[b, h, j], y_send.at[b, h, j], y_recv.at[b, h, j], "tp", pair_t)

    def reduce_along_z(b, h):
        for j, z in enumerate([*peers, me_z]):
            remote(
                terms.at[b, h, j], pair_terms.at[b, h, j], y_send.at[b, h, j], y_recv.at[b, h, j], "tp", pair_t
            ).wait_recv()
            if j < n_z - 1:
                mid_terms[b, h, j] = (acc[h, :, columns_of(2 * z + me_y)] + pair_terms[b, h, j].astype(F32)).astype(BF16)
                start(
                    mid_terms.at[b, h, j], terms_recv.at[b, h, me_z], t_send.at[b, h, j], t_recv.at[b, h, me_z],
                    "tp", 2 * z + me_y,
                )

    def residual(b, h):
        total = acc[h, :, columns_of(me_t)] + pair_terms[b, h, n_z - 1].astype(F32)
        for j, z in near_first:
            remote(
                mid_terms.at[b, h, j], terms_recv.at[b, h, z], t_send.at[b, h, j], t_recv.at[b, h, z],
                "tp", 2 * z + me_y,
            ).wait_recv()
            total = total + terms_recv[b, h, z].astype(F32)
        x_next = (xg[b, h, me_t].astype(F32) + total).astype(BF16)
        if b + 1 < BLOCKS:
            xg[b + 1, h, me_t] = x_next
            gather_send(b + 1, h)
        else:
            for d in range(n_dp):
                out_ref[pl.ds(d * own + h * half, half), :] = x_next[d * half:(d + 1) * half]

    pending = []

    def update(count):
        for b, h, head in pending[:count]:
            lanes = slice(head * HEAD_DIM, (head + 1) * HEAD_DIM)
            f = forget_ref[b, h, :, lanes].T
            for s in range(half):
                v = value_ref[b, h, s:s + 1, lanes]
                old = s_buf[b, h * half + s, head]
                s_buf[b, h * half + s, head] = v + f[:, s:s + 1] * (old - v)
        del pending[:count]

    both = range(HALVES)
    for h in both:
        gather_send(0, h)
    for c in loads[0][ROLES:]:
        c.start()
    for b in range(BLOCKS):
        for h in both:
            gather_along_z(b, h)
        for h in both:
            gather_along_y(b, h)
            for r in range(ROLES):
                project(b, h, r)
            if h:
                for r in range(ROLES):
                    between_chips(b, h - 1, r)
        for r in range(ROLES):
            between_chips(b, HALVES - 1, r)
        if b + 1 < BLOCKS:
            for c in loads[b + 1]:
                c.start()
        for h in both:
            read_out(b, h)
            pending += [(b, h, head) for head in range(heads)]
        units = len(pending)
        for h in both:
            mix(b, h)
        update(units // 4)
        for h in both:
            reduce_along_z(b, h)
        update(units // 2 if b + 1 < BLOCKS else units)
        for h in both:
            residual(b, h)
        update(units)
    for c in sends:
        c.wait_send()


def flush_kernel(x_ref, state_ref, out_ref, new_ref, sem):
    blocks, rows = state_ref.shape[:2]
    copies = [pltpu.make_async_copy(x_ref, out_ref, sem.at[0, 0])]
    for b in range(blocks):
        for c in range(PIECES):
            part = pl.ds(c * (rows // PIECES), rows // PIECES)
            copies.append(pltpu.make_async_copy(state_ref.at[b, part], new_ref.at[b, part], sem.at[1 + b, c]))
    for c in copies:
        c.start()
    for c in copies:
        c.wait()


def fast_body(
    n_tp, n_dp, residual, norm_gain, w_query, w_forget, w_value, w_output_gate, lower_bound, head_gain, w_out, state
):
    batch, feats = residual.shape
    rows, cols = w_query.shape[1:]
    own, heads = state.shape[1:3]
    half, many, n_z, each = own // HALVES, batch // HALVES, n_tp // 2, (BLOCKS, HALVES)
    vmem = pl.BlockSpec(memory_space=pltpu.VMEM)
    hbm = pl.BlockSpec(memory_space=pltpu.HBM)
    dma = pltpu.SemaphoreType.DMA
    current, fresh = pl.pallas_call(
        functools.partial(step_kernel, n_tp, n_dp),
        out_shape=(pltpu.VMEM((batch, feats), BF16), pltpu.VMEM(state.shape, F32)),
        in_specs=[hbm] * 10,
        out_specs=(vmem,) * 2,
        scratch_shapes=[
            pltpu.VMEM(norm_gain.shape, norm_gain.dtype),
            pltpu.VMEM(lower_bound.shape, lower_bound.dtype),
            pltpu.VMEM(head_gain.shape, head_gain.dtype),
            pltpu.VMEM((8, feats), F32),
            pltpu.VMEM((*each, half, cols), F32),
            pltpu.VMEM((*each, half, cols), F32),
            pltpu.VMEM((BLOCKS, ROLES, rows, cols), BF16),
            pltpu.VMEM((BLOCKS, *w_out.shape[1:]), BF16),
            pltpu.VMEM((*each, n_tp, many, feats), BF16),
            pltpu.VMEM((n_tp, 8, feats), F32),
            pltpu.VMEM((HALVES, many, rows), BF16),
            pltpu.VMEM((HALVES, many, feats), F32),
            pltpu.VMEM((*each, n_dp, half, LANES), F32),
            pltpu.VMEM((*each, n_dp, half, LANES), F32),
            pltpu.VMEM((*each, ROLES, n_dp, half, cols), BF16),
            pltpu.VMEM((*each, ROLES, n_dp // 2, half, cols), BF16),
            pltpu.VMEM((*each, ROLES, n_dp // 2, half, cols), BF16),
            pltpu.VMEM((*each, ROLES, n_dp, half, cols), BF16),
            pltpu.VMEM((HALVES, half, cols), F32),
            pltpu.VMEM((HALVES, half, cols), F32),
            pltpu.VMEM((*each, n_dp, half, cols), BF16),
            pltpu.VMEM((HALVES, many, n_tp * feats), F32),
            pltpu.VMEM((*each, n_z, many, feats), BF16),
            pltpu.VMEM((*each, n_z, many, feats), BF16),
            pltpu.VMEM((*each, n_z, many, feats), BF16),
            pltpu.VMEM((*each, n_z, many, feats), BF16),
            dma((HALVES * n_dp + 3,)),
            dma((BLOCKS, ROLES + 2)),
            dma((*each, n_tp)), dma((*each, n_tp)),
            dma((n_tp,)), dma((n_tp,)),
            dma((*each, n_dp)), dma((*each, n_dp)),
            dma((*each, ROLES, n_dp // 2)), dma((*each, ROLES, n_dp // 2)),
            dma((*each, ROLES, n_dp)), dma((*each, ROLES, n_dp)),
            dma((*each, n_dp)), dma((*each, n_dp)),
            dma((*each, n_z)), dma((*each, n_z)),
            dma((*each, n_z)), dma((*each, n_z)),
        ],
        compiler_params=pltpu.CompilerParams(
            collective_id=0, has_side_effects=True, vmem_limit_bytes=32 * 1024 * 1024
        ),
        name="recurrent_step",
    )(
        *(
            pltpu.with_memory_space_constraint(a, pltpu.HBM)
            for a in (
                residual, norm_gain, lower_bound, head_gain, w_query, w_forget, w_value, w_output_gate, w_out, state
            )
        )
    )
    return tuple(pl.pallas_call(
        flush_kernel,
        out_shape=(jax.ShapeDtypeStruct((batch, feats), BF16), jax.ShapeDtypeStruct(state.shape, F32)),
        in_specs=[vmem] * 2,
        out_specs=(hbm,) * 2,
        scratch_shapes=[dma((1 + BLOCKS, PIECES))],
        compiler_params=pltpu.CompilerParams(vmem_limit_bytes=4 * 1024 * 1024),
        name="flush",
    )(
        pltpu.with_memory_space_constraint(current, pltpu.VMEM),
        pltpu.with_memory_space_constraint(fresh, pltpu.VMEM),
    ))


def solution(mesh):
    placed = (
        P(None, ("dp", "tp")),
        P(None, ("dp", "tp")),
        P(None, "dp", "tp"),
        P(None, "dp", "tp"),
        P(None, "dp", "tp"),
        P(None, "dp", "tp"),
        P(None, "tp"),
        P(None, "tp"),
        P(None, "tp", "dp"),
        P(None, "dp", "tp", None, None),
    )
    n_tp, n_dp = mesh.shape["tp"], mesh.shape["dp"]
    whole_tiles = D % (n_tp * n_dp * LANES) == 0 and n_tp in (2, 4, 8, 16) and n_dp % 2 == 0
    return jax.shard_map(
        functools.partial(fast_body, n_tp, n_dp) if whole_tiles else body,
        mesh=mesh,
        in_specs=placed,
        out_specs=(P(None, ("dp", "tp")), P(None, "dp", "tp", None, None)),
        check_vma=False,
    )
```

time: 76.9 us -> 64.9 us (0.84)
  Pallas kernels: 76.1 us -> 64 us
    pallas_call x1, Pallas kernels: 70 us -> 58 us  [fast_body(): pl.pallas_call(functools.partial(step_kernel, n_tp, n_dp), out_shape=(plt...]
where the time goes in v2:
time: 64.9 us; the launch traced here: 64.7 us
  Pallas kernels  64 us (99%)
    pallas_call x1, Pallas kernels, fast_body(): pl.pallas_call(functools.partial(step_kernel, n_tp, n_dp), out_shape=(plt...  58 us
    pallas_call x1, Pallas kernels, fast_body(): pl.pallas_call(flush_kernel, out_shape=(jax.ShapeDtypeStruct((batch, feat...  6.04 us

profile of v2, /device:TPU:0, one launch (start us, length us, event | category | flops | bytes accessed | tf_op | source)
XLA Modules:
  0.0 64.7 jit_solution(4781400571734869686)
XLA Ops:
  0.6 58.0 %recurrent_step.1 = (bf16[128,128]{1,0:T(8,128)(2,1)S(1)}, f32[2,32,4,128,128]{4,3,2,1,0:T(8,128)S(1)}) custom-call(bf16[128,128]{1,0:T(8,128)(2,1)} %x_hbm.1, bf16[2,128]{1,0:T(2,128)(2,1)} %gain_hbm.1, f32[2,512]{1,0:T(2,128)} %bound_hbm.1, bf16[2,512]{1,0:T(2,128)(2,1)} %h_gain_hbm.1, bf16[2,1024,512]{2,1,0:T(8,128)(2,1)} %wq_hbm.1, ...), custom_call_target="tpu_custom_call" | custom-call | tf_op jit(solution)/shard_map/recurrent_step/pallas_call | solution.py:445
  58.6 6.0 %flush.1 = (bf16[128,128]{1,0:T(8,128)(2,1)}, f32[2,32,4,128,128]{4,3,2,1,0:T(8,128)}) custom-call(bf16[128,128]{1,0:T(8,128)(2,1)S(1)} %get-tuple-element.4.x_ref, f32[2,32,4,128,128]{4,3,2,1,0:T(8,128)S(1)} %get-tuple-element.5.state_ref), custom_call_target="tpu_custom_call" | custom-call | tf_op jit(solution)/shard_map/flush/pallas_call | solution.py:500
